TPU v7x, 32 devices: a whole 2x2x4 slice. The times are simulated.
32 devices in a mesh: grp: 2 (over y), sp: 8 (over z, x), tp: 2 (over core).
Axes of the slice: x: 2, y: 2, z: 4, core: 2. Of those that a mesh axis runs over, the one named last changes fastest.
Arguments:
- layer_input: bfloat16 [4, 1024, 2048], P('grp', ('sp', 'tp')), parts along dimension 0, may hold values from -6 to 6
- norm_gain: float32 [2048], replicated, may hold values from 0.1 to 1.9
- in_weight: bfloat16 [2048, 1024], P(None, 'tp'), may hold values from -0.125 to 0.125
- gate_weight: bfloat16 [2048, 1024], P(None, 'tp'), may hold values from -0.125 to 0.125
- rate_real: float32 [64, 64], P('tp'), may hold values from -1 to 0
- rate_imag: float32 [64, 64], P('tp'), may hold values from -3 to 3
- log_step: float32 [64], P('tp'), may hold values from -8 to -2.5
- input_real: bfloat16 [64, 64, 16], P('tp'), may hold values from -4 to 4
- input_imag: bfloat16 [64, 64, 16], P('tp'), may hold values from -4 to 4
- output_real: bfloat16 [64, 16, 64], P('tp'), may hold values from -10 to 10
- output_imag: bfloat16 [64, 16, 64], P('tp'), may hold values from -10 to 10
- skip_weight: float32 [1024], P('tp'), may hold values from -20 to 20
- decay_offset: float32 [4, 1024, 64], P('grp', 'sp', 'tp'), parts along dimension 0, may hold values from -1.5 to 0
- channel_gain: float32 [1024], replicated, may hold values from 0.1 to 1.9
- out_weight: bfloat16 [1024, 2048], P('tp'), may hold values from -0.1875 to 0.1875
Outputs:
- layer_output: bfloat16 [4, 1024, 2048], P('grp', ('sp', 'tp')), parts along dimension 0
There are 2 independent parts, one for each index of `grp`. A program takes and returns all parts, laid end to end along the dimension named above; an argument that names none is the same for every part. Nothing has to cross between parts.
All inputs are finite; a program needn't handle non-finite values.
Results may differ from a plain program's by a relative error of at most 0.014.
Values may be sent and summed in bfloat16 or wider, within the bound.
A program may use at most 128 MiB of HBM per device.

v0:
```python
import functools

import jax
import jax.numpy as jnp
from jax import lax
from jax.experimental import pallas as pl
from jax.experimental.pallas import tpu as pltpu
from jax.sharding import PartitionSpec as P

epsilon = 1e-06
HIGHEST = lax.Precision.HIGHEST
MESH = pl.DeviceIdType.MESH
F32 = jnp.float32
BF16 = jnp.bfloat16


def iota(shape, dim):
    return lax.broadcasted_iota(jnp.int32, shape, dim)


def cmul(a, b):
    return (a[0] * b[0] - a[1] * b[1], a[0] * b[1] + a[1] * b[0])


def cpow(a, k):
    result = None
    while k:
        if k & 1:
            result = a if result is None else cmul(result, a)
        k >>= 1
        if k:
            a = cmul(a, a)
    return result


def dot(a, b, precision=None):
    return jnp.dot(a, b, preferred_element_type=F32, precision=precision)


def dot_nt(a, b):
    return lax.dot_general(a, b, (((1,), (1,)), ((), ())), preferred_element_type=F32)


def kernel(
    sizes,
    x_hbm, ng, inw_hbm, gw_hbm, rr, ri, ls, bre, bim, cre, cim, skip, dec, cg, outw_hbm,
    out,
    xf, w_in, w_g, w_o, nrm, u_ref, gate_ref, rel_ref,
    bd_re, bd_im, cd_re, cd_im, ti_re, ti_im, to_re, to_im,
    p_re, p_im, xc_re, xc_im, tot, tot_all, st, st_all, act, act_in,
    load_sem, tp_send, tp_recv, tot_send, tot_recv, st_send, st_recv,
):
    n, tp, S, Q, D, G, N, C, tile_g, out_cols = sizes
    W = G * C
    tiles = G // tile_g
    cw, mw = tile_g * C, tile_g * N
    SQ = S * Q
    mid = Q // 2 - 1
    sp_me = lax.axis_index("sp")
    me = lax.axis_index("tp")
    peer = 1 - me

    barrier = pltpu.get_barrier_semaphore()
    pl.semaphore_signal(barrier, inc=1, device_id={"tp": peer}, device_id_type=MESH)

    def greet(i, carry):
        other = lax.rem(sp_me + 1 + i, n)
        pl.semaphore_signal(barrier, inc=1, device_id={"sp": other}, device_id_type=MESH)
        return carry

    lax.fori_loop(0, n - 1, greet, 0)

    load_x = pltpu.make_async_copy(x_hbm, xf.at[me], load_sem.at[0])
    load_in = pltpu.make_async_copy(inw_hbm, w_in, load_sem.at[1])
    load_g = pltpu.make_async_copy(gw_hbm, w_g, load_sem.at[2])
    load_o = pltpu.make_async_copy(outw_hbm, w_o.at[me], load_sem.at[3])
    load_x.start()
    load_in.start()
    load_g.start()
    load_o.start()

    tri = (iota((Q, Q), 0) >= iota((Q, Q), 1)).astype(F32)
    to_chan = (iota((G, W), 1) // C == iota((G, W), 0)).astype(F32)
    mids, lasts, totals = [], [], []
    tot[...] = jnp.zeros_like(tot)
    for s in range(S):
        total = None
        for c in range(tp):
            cum = dot(tri, dec[s, c * Q:(c + 1) * Q, :], HIGHEST)
            at_mid = cum[mid:mid + 1, :]
            at_end = cum[Q - 1:Q, :]
            mids.append(at_mid)
            lasts.append(at_end - at_mid)
            total = at_end if total is None else total + at_end
            rows = (c * S + s) * Q
            rel_ref[rows:rows + Q, :] = dot(cum - at_mid, to_chan, HIGHEST)
        totals.append(total)
        tot[s:s + 1, :] = total

    pl.semaphore_wait(barrier, n)

    load_x.wait()
    load_o.wait()
    send_x = pltpu.make_async_remote_copy(
        xf.at[me], xf.at[me], tp_send.at[0], tp_recv.at[0], device_id={"tp": peer}, device_id_type=MESH
    )
    send_o = pltpu.make_async_remote_copy(
        w_o.at[me], w_o.at[me], tp_send.at[1], tp_recv.at[1], device_id={"tp": peer}, device_id_type=MESH
    )
    send_x.start()
    send_o.start()

    def tot_copy(target):
        return pltpu.make_async_remote_copy(
            tot, tot_all.at[sp_me], tot_send.at[target], tot_recv.at[sp_me],
            device_id={"sp": target}, device_id_type=MESH,
        )

    def st_copy(target):
        return pltpu.make_async_remote_copy(
            st, st_all.at[sp_me], st_send.at[target], st_recv.at[sp_me],
            device_id={"sp": target}, device_id_type=MESH,
        )

    def to_later(act_on):
        def body(i, carry):
            act_on(n - 1 - i)
            return carry

        lax.fori_loop(0, n - 1 - sp_me, body, 0)

    to_later(lambda target: tot_copy(target).start())

    ls_row = jnp.broadcast_to(ls[...], (G, G))
    step = jnp.exp(jnp.sum(jnp.where(iota((G, G), 0) == iota((G, G), 1), ls_row, 0.0), axis=1, keepdims=True))
    rate_re, rate_im = rr[...], ri[...]
    real_step = rate_re * step
    angle_step = rate_im * step
    cosa, sina = jnp.cos(angle_step), jnp.sin(angle_step)
    half = jnp.sin(0.5 * angle_step)
    grown = jnp.exp(real_step)
    shrunk = jnp.exp(-real_step)
    series = jnp.ones_like(real_step)
    for k in range(11, 1, -1):
        series = 1.0 + real_step * (1.0 / k) * series
    minus_one = jnp.where(jnp.abs(real_step) < 0.5, real_step * series, grown - 1.0)
    top_re = minus_one * cosa - 2.0 * half * half
    top_im = grown * sina
    inverse = 1.0 / (rate_re * rate_re + rate_im * rate_im)
    coef_re = (top_re * rate_re + top_im * rate_im) * inverse
    coef_im = (top_im * rate_re - top_re * rate_im) * inverse
    spread = (iota((N, mw), 1) % N == iota((N, mw), 0)).astype(F32)
    to_mode = (iota((tile_g, mw), 1) // N == iota((tile_g, mw), 0)).astype(F32)

    def rows_of(item, q):
        wide = dot(item[q * tile_g:(q + 1) * tile_g, :], spread, HIGHEST)
        return jnp.sum(wide * to_mode, axis=0, keepdims=True)

    up_half, up_end, up_all = [], [], []
    k8 = iota((8, mw), 0)
    bmask = iota((mw, cw), 0) // N == iota((mw, cw), 1) // C
    cmask = iota((cw, mw), 0) // C == iota((cw, mw), 1) // N
    btile = (iota((C, cw), 1) % C == iota((C, cw), 0)).astype(BF16)
    ctile = spread.astype(BF16)

    def table(a, base, t_re, t_im, q):
        a2 = cmul(a, a)
        a4 = cmul(a2, a2)
        a8 = cmul(a4, a4)
        block = tuple(jnp.broadcast_to(b, (8, mw)) for b in base)
        for bit, power in ((1, a), (2, a2), (4, a4)):
            on = (k8 & bit) != 0
            block = cmul(block, (jnp.where(on, power[0], 1.0), jnp.where(on, power[1], 0.0)))
        for j in range(Q // 8):
            t_re[q, j * 8:j * 8 + 8, :] = block[0]
            t_im[q, j * 8:j * 8 + 8, :] = block[1]
            block = cmul(block, a8)

    for q in range(tiles):
        a = (rows_of(grown * cosa, q), rows_of(grown * sina, q))
        inv = (rows_of(shrunk * cosa, q), rows_of(-shrunk * sina, q))
        coef = (rows_of(coef_re, q), rows_of(coef_im, q))
        table(inv, cmul(coef, cpow(a, mid)), ti_re, ti_im, q)
        table(a, cpow(inv, mid), to_re, to_im, q)
        up_half.append(cpow(a, mid + 1))
        up_end.append(cpow(a, Q - 1 - mid))
        up_all.append(cpow(a, Q * tp))
        for src, dst in ((bre, bd_re), (bim, bd_im)):
            dst[q] = jnp.where(bmask, dot(src[q * mw:(q + 1) * mw, :], btile), 0.0).astype(BF16)
        for src, dst in ((cre, cd_re), (cim, cd_im)):
            dst[q] = jnp.where(cmask, dot(src[q * cw:(q + 1) * cw, :], ctile), 0.0).astype(BF16)

    row_tile = min(32, Q)

    def project(slot):
        first = slot * SQ

        def normalize(i, carry):
            s = i // (Q // row_tile)
            r = pl.multiple_of((i % (Q // row_tile)) * row_tile, row_tile)
            x = xf[slot, s, pl.ds(r, row_tile), :].astype(F32)
            scale = lax.rsqrt(jnp.mean(x * x, axis=-1, keepdims=True) + epsilon)
            rows = pl.ds(pl.multiple_of(first + i * row_tile, row_tile), row_tile)
            nrm[rows, :] = (x * scale * ng[...]).astype(BF16)
            return carry

        lax.fori_loop(0, SQ // row_tile, normalize, 0)
        rows = pl.ds(pl.multiple_of(first, SQ), SQ)
        u_ref[rows, :] = dot(nrm[rows, :], w_in[...]).astype(BF16)

    load_in.wait()
    project(me)
    send_x.wait_recv()
    project(peer)

    R = tp * SQ
    ri_, ci_ = iota((R, R), 0), iota((R, R), 1)
    chunk_tri = ((ri_ >= ci_) & (ri_ // Q == ci_ // Q)).astype(BF16)

    for q in range(tiles):
        cols = slice(q * cw, (q + 1) * cw)
        uq = (u_ref[:, cols].astype(F32) * jnp.exp(-rel_ref[:, cols])).astype(BF16)
        d_re = dot_nt(uq, bd_re[q]).reshape(tp * S, Q, mw)
        d_im = dot_nt(uq, bd_im[q]).reshape(tp * S, Q, mw)
        t = (ti_re[q][None], ti_im[q][None])
        z_re, z_im = cmul(t, (d_re, d_im))
        p_re[q] = dot(chunk_tri, z_re.reshape(R, mw).astype(BF16))
        p_im[q] = dot(chunk_tri, z_im.reshape(R, mw).astype(BF16))

    def widen(row, q):
        return jnp.exp(dot(jnp.broadcast_to(row[:, q * tile_g:(q + 1) * tile_g], (8, tile_g)), to_mode, HIGHEST)[0:1])

    enter_f, leave_f = {}, {}
    for q in range(tiles):
        for s in range(S):
            x = None
            for c in range(tp):
                b = c * S + s
                e_mid = widen(mids[s * tp + c], q)
                e_end = widen(lasts[s * tp + c], q)
                enter_f[q, s, c] = (up_half[q][0] * e_mid, up_half[q][1] * e_mid)
                leave_f[q, s, c] = (up_end[q][0] * e_end, up_end[q][1] * e_end)
                last = b * Q + Q - 1
                end = (p_re[q, last:last + 1, :], p_im[q, last:last + 1, :])
                if x is not None:
                    add = cmul(enter_f[q, s, c], x)
                    end = (end[0] + add[0], end[1] + add[1])
                x = cmul(leave_f[q, s, c], end)
            st[q, s:s + 1, :] = x[0].astype(BF16)
            st[q, S + s:S + s + 1, :] = x[1].astype(BF16)

    to_later(lambda target: st_copy(target).start())

    load_g.wait()
    gate_ref[...] = dot(nrm[...], w_g[...]).astype(BF16)

    def enter(j, x):
        pltpu.make_async_remote_copy(
            tot, tot_all.at[j], tot_send.at[j], tot_recv.at[j], device_id={"tp": peer}, device_id_type=MESH
        ).wait_recv()
        pltpu.make_async_remote_copy(
            st, st_all.at[j], st_send.at[j], st_recv.at[j], device_id={"tp": peer}, device_id_type=MESH
        ).wait_recv()
        logs = tot_all[j]
        new = []
        for q in range(tiles):
            decay = jnp.exp(dot(logs[:, q * tile_g:(q + 1) * tile_g], to_mode, HIGHEST))[0:S]
            got = st_all[j, q].astype(F32)
            re, im = cmul((up_all[q][0] * decay, up_all[q][1] * decay), x[q])
            new.append((re + got[0:S], im + got[S:2 * S]))
        return tuple(new)

    zero = jnp.zeros((S, mw), F32)
    entering = lax.fori_loop(0, sp_me, enter, tuple((zero, zero) for _ in range(tiles)))

    for q in range(tiles):
        for s in range(S):
            x = (entering[q][0][s:s + 1], entering[q][1][s:s + 1])
            for c in range(tp):
                b = c * S + s
                add = cmul(enter_f[q, s, c], x)
                xc_re[q, b:b + 1, :] = add[0]
                xc_im[q, b:b + 1, :] = add[1]
                if c < tp - 1:
                    last = b * Q + Q - 1
                    x = cmul(
                        leave_f[q, s, c],
                        (p_re[q, last:last + 1, :] + add[0], p_im[q, last:last + 1, :] + add[1]),
                    )

    def read_out(slot, dst):
        first = pl.multiple_of(slot * SQ, SQ)
        rows = pl.ds(first, SQ)
        for q in range(tiles):
            cols = slice(q * cw, (q + 1) * cw)
            acc_re, acc_im = [], []
            for s in range(S):
                block = pl.ds(pl.multiple_of(first + s * Q, Q), Q)
                one = pl.ds(slot * S + s, 1)
                v = (p_re[q, block, :] + xc_re[q, one, :], p_im[q, block, :] + xc_im[q, one, :])
                w = cmul((to_re[q], to_im[q]), v)
                acc_re.append(w[0].astype(BF16))
                acc_im.append(w[1].astype(BF16))
            w_re = jnp.concatenate(acc_re, axis=0)
            w_im = jnp.concatenate(acc_im, axis=0)
            y = dot_nt(w_re, cd_re[q]) - dot_nt(w_im, cd_im[q])
            mixed = y * jnp.exp(rel_ref[rows, cols]) + skip[:, cols] * u_ref[rows, cols].astype(F32)
            gate = jax.nn.sigmoid(gate_ref[rows, cols].astype(F32))
            gelu = 0.5 * mixed * (1.0 + lax.erf(mixed * 0.7071067811865476))
            dst[:, cols] = (gelu * gate).astype(BF16)

    read_out(peer, act.at[peer])
    send_a = pltpu.make_async_remote_copy(
        act.at[peer], act_in, tp_send.at[2], tp_recv.at[2], device_id={"tp": peer}, device_id_type=MESH
    )
    send_a.start()
    read_out(me, act.at[me])
    own = act[me].astype(F32)
    own_sq = jnp.sum(own * own, axis=-1, keepdims=True)
    own_g = (own * cg[me]).astype(BF16)
    send_o.wait_recv()
    send_a.wait_recv()
    got = act_in[...].astype(F32)
    got_sq = jnp.sum(got * got, axis=-1, keepdims=True)
    got_g = (got * cg[peer]).astype(BF16)
    scale = lax.rsqrt((own_sq + got_sq) * (1.0 / (tp * W)) + epsilon)
    for k in range(D // out_cols):
        cols = slice(k * out_cols, (k + 1) * out_cols)
        y = dot(own_g, w_o[me, :, cols]) + dot(got_g, w_o[peer, :, cols])
        out[:, :, cols] = (y * scale).astype(BF16).reshape(S, Q, out_cols)

    send_x.wait_send()
    send_o.wait_send()
    send_a.wait_send()
    to_later(lambda target: tot_copy(target).wait_send())
    to_later(lambda target: st_copy(target).wait_send())


def shards(
    n, tp, layer_input, norm_gain, in_weight, gate_weight, rate_real, rate_imag, log_step, input_real,
    input_imag, output_real, output_imag, skip_weight, decay_offset, channel_gain, out_weight,
):
    S, Q, D = layer_input.shape
    G, N = rate_real.shape
    C = input_real.shape[2]
    W = G * C
    tile_g = min(G, max(1, 128 // C))
    tiles = G // tile_g
    cw, mw = tile_g * C, tile_g * N
    R = tp * S * Q
    assert tp == 2 and Q <= 64 and Q % 8 == 0
    sizes = (n, tp, S, Q, D, G, N, C, tile_g, min(512, D))
    vmem = pl.BlockSpec(memory_space=pltpu.VMEM)
    hbm = pl.BlockSpec(memory_space=pl.ANY)
    dma = pltpu.SemaphoreType.DMA
    return pl.pallas_call(
        functools.partial(kernel, sizes),
        out_shape=jax.ShapeDtypeStruct((S, Q, D), BF16),
        in_specs=[hbm, vmem, hbm, hbm] + [vmem] * 10 + [hbm],
        out_specs=vmem,
        scratch_shapes=[
            pltpu.VMEM((tp, S, Q, D), BF16),
            pltpu.VMEM((D, W), BF16),
            pltpu.VMEM((D, W), BF16),
            pltpu.VMEM((tp, W, D), BF16),
            pltpu.VMEM((R, D), BF16),
            pltpu.VMEM((R, W), BF16),
            pltpu.VMEM((R, W), BF16),
            pltpu.VMEM((R, W), F32),
            pltpu.VMEM((tiles, mw, cw), BF16),
            pltpu.VMEM((tiles, mw, cw), BF16),
            pltpu.VMEM((tiles, cw, mw), BF16),
            pltpu.VMEM((tiles, cw, mw), BF16),
            pltpu.VMEM((tiles, Q, mw), F32),
            pltpu.VMEM((tiles, Q, mw), F32),
            pltpu.VMEM((tiles, Q, mw), F32),
            pltpu.VMEM((tiles, Q, mw), F32),
            pltpu.VMEM((tiles, R, mw), F32),
            pltpu.VMEM((tiles, R, mw), F32),
            pltpu.VMEM((tiles, tp * S, mw), F32),
            pltpu.VMEM((tiles, tp * S, mw), F32),
            pltpu.VMEM((8, G), F32),
            pltpu.VMEM((n, 8, G), F32),
            pltpu.VMEM((tiles, 2 * S, mw), BF16),
            pltpu.VMEM((n, tiles, 2 * S, mw), BF16),
            pltpu.VMEM((tp, S * Q, W), BF16),
            pltpu.VMEM((S * Q, W), BF16),
            dma((4,)),
            dma((3,)),
            dma((3,)),
            dma((n,)),
            dma((n,)),
            dma((n,)),
            dma((n,)),
        ],
        compiler_params=pltpu.CompilerParams(
            collective_id=0, has_side_effects=True, vmem_limit_bytes=60 * 1024 * 1024
        ),
    )(
        layer_input,
        norm_gain.reshape(1, D),
        in_weight,
        gate_weight,
        rate_real,
        rate_imag,
        log_step.reshape(1, G),
        input_real.reshape(G * N, C),
        input_imag.reshape(G * N, C),
        output_real.reshape(G * C, N),
        output_imag.reshape(G * C, N),
        skip_weight.reshape(1, W),
        decay_offset,
        channel_gain.reshape(tp, 1, W),
        out_weight,
    )


def solution(mesh):
    placed = (
        P("grp", ("sp", "tp"), None),
        P(),
        P(None, "tp"),
        P(None, "tp"),
        P("tp", None),
        P("tp", None),
        P("tp"),
        P("tp", None, None),
        P("tp", None, None),
        P("tp", None, None),
        P("tp", None, None),
        P("tp"),
        P("grp", "sp", "tp"),
        P(),
        P("tp", None),
    )
    body = functools.partial(shards, mesh.shape["sp"], mesh.shape["tp"])
    return jax.shard_map(
        body, mesh=mesh, in_specs=placed, out_specs=P("grp", ("sp", "tp"), None), check_vma=False
    )
```

profile of v0, /device:TPU:17, one launch (start us, length us, event | category | flops | bytes accessed | tf_op | source)
XLA Modules:
  0.0 28.3 jit_solution(17752703003781647205)
XLA Ops:
  0.0 1.5 %copy.18.dec = f32[2,128,32]{2,1,0:T(8,128)} copy(f32[2,128,32]{1,2,0:T(8,128)} %param.27) | data formatting | bytes 65536 | tf_op args[12]
  1.5 1.9 %copy.16 = bf16[32,64,16]{2,1,0:T(8,128)(2,1)} copy(bf16[32,64,16]{1,2,0:T(8,128)(2,1)} %param.22) | data formatting | bytes 131072 | tf_op args[7]
  3.4 1.9 %copy.17 = bf16[32,64,16]{2,1,0:T(8,128)(2,1)} copy(bf16[32,64,16]{1,2,0:T(8,128)(2,1)} %param.23) | data formatting | bytes 131072 | tf_op args[8]
  5.3 21.1 %shard_map.145 = bf16[2,64,2048]{2,1,0:T(8,128)(2,1)} custom-call(bf16[2,64,2048]{2,1,0:T(8,128)(2,1)} %x_hbm.1, f32[1,2048]{1,0:T(1,128)} %bitcast.12, bf16[2048,512]{1,0:T(8,128)(2,1)} %inw_hbm.1, bf16[2048,512]{1,0:T(8,128)(2,1)} %gw_hbm.1, f32[32,64]{1,0:T(8,128)} %rr.1, f32[32,64]{1,0:T(8,128)} %ri.1, f32[1,32]{1,0:T(1,128)} %bitcast.15, ...), custom_call_target="tpu_custom_call" | custom-call | tf_op jit(solution)/shard_map/pallas_call | solution.py:356
  26.4 1.9 %copy.20 = bf16[2,64,2048]{2,1,0:T(8,128)(2,1)} copy(bf16[2,64,2048]{2,1,0:T(8,128)(2,1)} %shard_map.145) | data formatting | bytes 1048576
where the time goes:
time: 28.8 us; the launch traced here: 28.3 us
  Pallas kernels  21.1 us (73%)
  local copies, waits for them, and re-layouts  7.21 us (25%)
    pallas_call x1, Pallas kernels, shards(): pl.pallas_call(functools.partial(kernel, sizes), out_shape=jax.ShapeDtype...  21.1 us
    unnamed x4, local copies, waits for them, and re-layouts  7.21 us

commit v1 on v0

--- a/solution.py
+++ b/solution.py
@@ -37,18 +37,20 @@
     return jnp.dot(a, b, preferred_element_type=F32, precision=precision)
 
 
-def dot_nt(a, b):
-    return lax.dot_general(a, b, (((1,), (1,)), ((), ())), preferred_element_type=F32)
+def dot_nt(a, b, precision=None):
+    return lax.dot_general(a, b, (((1,), (1,)), ((), ())), preferred_element_type=F32, precision=precision)
 
 
 def kernel(
     sizes,
-    x_hbm, ng, inw_hbm, gw_hbm, rr, ri, ls, bre, bim, cre, cim, skip, dec, cg, outw_hbm,
+    x_hbm, ng_hbm, inw_hbm, gw_hbm, rr_hbm, ri_hbm, ls_hbm, bre_hbm, bim_hbm, cre_hbm, cim_hbm,
+    skip_hbm, dec_hbm, cg_hbm, outw_hbm,
     out,
+    ng, rr, ri, ls, bre, bim, cre, cim, skip, dec, cg,
     xf, w_in, w_g, w_o, nrm, u_ref, gate_ref, rel_ref,
     bd_re, bd_im, cd_re, cd_im, ti_re, ti_im, to_re, to_im,
     p_re, p_im, xc_re, xc_im, tot, tot_all, st, st_all, act, act_in,
-    load_sem, tp_send, tp_recv, tot_send, tot_recv, st_send, st_recv,
+    load_sem, small_sem, tp_send, tp_recv, tot_send, tot_recv, st_send, st_recv,
 ):
     n, tp, S, Q, D, G, N, C, tile_g, out_cols = sizes
     W = G * C
@@ -74,11 +76,21 @@
     load_in = pltpu.make_async_copy(inw_hbm, w_in, load_sem.at[1])
     load_g = pltpu.make_async_copy(gw_hbm, w_g, load_sem.at[2])
     load_o = pltpu.make_async_copy(outw_hbm, w_o.at[me], load_sem.at[3])
+    small = [
+        pltpu.make_async_copy(src, dst, small_sem.at[i])
+        for i, (src, dst) in enumerate((
+            (dec_hbm, dec), (ls_hbm, ls), (rr_hbm, rr), (ri_hbm, ri), (bre_hbm, bre), (bim_hbm, bim),
+            (cre_hbm, cre), (cim_hbm, cim), (ng_hbm, ng), (skip_hbm, skip), (cg_hbm, cg),
+        ))
+    ]
     load_x.start()
+    for copy in small:
+        copy.start()
     load_in.start()
     load_g.start()
     load_o.start()
 
+    small[0].wait()
     tri = (iota((Q, Q), 0) >= iota((Q, Q), 1)).astype(F32)
     to_chan = (iota((G, W), 1) // C == iota((G, W), 0)).astype(F32)
     mids, lasts, totals = [], [], []
@@ -86,7 +98,7 @@
     for s in range(S):
         total = None
         for c in range(tp):
-            cum = dot(tri, dec[s, c * Q:(c + 1) * Q, :], HIGHEST)
+            cum = dot_nt(tri, dec[s, :, c * Q:(c + 1) * Q], HIGHEST)
             at_mid = cum[mid:mid + 1, :]
             at_end = cum[Q - 1:Q, :]
             mids.append(at_mid)
@@ -131,6 +143,8 @@
 
     to_later(lambda target: tot_copy(target).start())
 
+    for copy in small[1:]:
+        copy.wait()
     ls_row = jnp.broadcast_to(ls[...], (G, G))
     step = jnp.exp(jnp.sum(jnp.where(iota((G, G), 0) == iota((G, G), 1), ls_row, 0.0), axis=1, keepdims=True))
     rate_re, rate_im = rr[...], ri[...]
@@ -158,9 +172,7 @@
 
     up_half, up_end, up_all = [], [], []
     k8 = iota((8, mw), 0)
-    bmask = iota((mw, cw), 0) // N == iota((mw, cw), 1) // C
     cmask = iota((cw, mw), 0) // C == iota((cw, mw), 1) // N
-    btile = (iota((C, cw), 1) % C == iota((C, cw), 0)).astype(BF16)
     ctile = spread.astype(BF16)
 
     def table(a, base, t_re, t_im, q):
@@ -185,9 +197,7 @@
         up_half.append(cpow(a, mid + 1))
         up_end.append(cpow(a, Q - 1 - mid))
         up_all.append(cpow(a, Q * tp))
-        for src, dst in ((bre, bd_re), (bim, bd_im)):
-            dst[q] = jnp.where(bmask, dot(src[q * mw:(q + 1) * mw, :], btile), 0.0).astype(BF16)
-        for src, dst in ((cre, cd_re), (cim, cd_im)):
+        for src, dst in ((bre, bd_re), (bim, bd_im), (cre, cd_re), (cim, cd_im)):
             dst[q] = jnp.where(cmask, dot(src[q * cw:(q + 1) * cw, :], ctile), 0.0).astype(BF16)
 
     row_tile = min(32, Q)
@@ -220,8 +230,8 @@
     for q in range(tiles):
         cols = slice(q * cw, (q + 1) * cw)
         uq = (u_ref[:, cols].astype(F32) * jnp.exp(-rel_ref[:, cols])).astype(BF16)
-        d_re = dot_nt(uq, bd_re[q]).reshape(tp * S, Q, mw)
-        d_im = dot_nt(uq, bd_im[q]).reshape(tp * S, Q, mw)
+        d_re = dot(uq, bd_re[q]).reshape(tp * S, Q, mw)
+        d_im = dot(uq, bd_im[q]).reshape(tp * S, Q, mw)
         t = (ti_re[q][None], ti_im[q][None])
         z_re, z_im = cmul(t, (d_re, d_im))
         p_re[q] = dot(chunk_tri, z_re.reshape(R, mw).astype(BF16))
@@ -351,14 +361,25 @@
     assert tp == 2 and Q <= 64 and Q % 8 == 0
     sizes = (n, tp, S, Q, D, G, N, C, tile_g, min(512, D))
     vmem = pl.BlockSpec(memory_space=pltpu.VMEM)
-    hbm = pl.BlockSpec(memory_space=pl.ANY)
+    hbm = pl.BlockSpec(memory_space=pltpu.HBM)
     dma = pltpu.SemaphoreType.DMA
     return pl.pallas_call(
         functools.partial(kernel, sizes),
         out_shape=jax.ShapeDtypeStruct((S, Q, D), BF16),
-        in_specs=[hbm, vmem, hbm, hbm] + [vmem] * 10 + [hbm],
+        in_specs=[hbm] * 15,
         out_specs=vmem,
         scratch_shapes=[
+            pltpu.VMEM((1, D), F32),
+            pltpu.VMEM((G, N), F32),
+            pltpu.VMEM((G, N), F32),
+            pltpu.VMEM((1, G), F32),
+            pltpu.VMEM((W, N), BF16),
+            pltpu.VMEM((W, N), BF16),
+            pltpu.VMEM((W, N), BF16),
+            pltpu.VMEM((W, N), BF16),
+            pltpu.VMEM((1, W), F32),
+            pltpu.VMEM((S, G, tp * Q), F32),
+            pltpu.VMEM((tp, 1, W), F32),
             pltpu.VMEM((tp, S, Q, D), BF16),
             pltpu.VMEM((D, W), BF16),
             pltpu.VMEM((D, W), BF16),
@@ -367,8 +388,8 @@
             pltpu.VMEM((R, W), BF16),
             pltpu.VMEM((R, W), BF16),
             pltpu.VMEM((R, W), F32),
-            pltpu.VMEM((tiles, mw, cw), BF16),
-            pltpu.VMEM((tiles, mw, cw), BF16),
+            pltpu.VMEM((tiles, cw, mw), BF16),
+            pltpu.VMEM((tiles, cw, mw), BF16),
             pltpu.VMEM((tiles, cw, mw), BF16),
             pltpu.VMEM((tiles, cw, mw), BF16),
             pltpu.VMEM((tiles, Q, mw), F32),
@@ -386,6 +407,7 @@
             pltpu.VMEM((tp, S * Q, W), BF16),
             pltpu.VMEM((S * Q, W), BF16),
             dma((4,)),
+            dma((11,)),
             dma((3,)),
             dma((3,)),
             dma((n,)),
@@ -404,12 +426,12 @@
         rate_real,
         rate_imag,
         log_step.reshape(1, G),
-        input_real.reshape(G * N, C),
-        input_imag.reshape(G * N, C),
+        jnp.swapaxes(input_real, 1, 2).reshape(G * C, N),
+        jnp.swapaxes(input_imag, 1, 2).reshape(G * C, N),
         output_real.reshape(G * C, N),
         output_imag.reshape(G * C, N),
         skip_weight.reshape(1, W),
-        decay_offset,
+        jnp.swapaxes(decay_offset, 1, 2),
         channel_gain.reshape(tp, 1, W),
         out_weight,
     )

time: 28.8 us -> 22 us (0.76)
  local copies, waits for them, and re-layouts: 7.21 us -> 1.88 us
  Pallas kernels: 21.1 us -> 19.9 us
    unnamed x4 -> x1, local copies, waits for them, and re-layouts: 7.21 us -> 1.88 us
    pallas_call x1, Pallas kernels: 21.1 us -> 19.9 us  [shards(): pl.pallas_call(functools.partial(kernel, sizes), out_shape=jax.ShapeDtype...]
where the time goes in v1:
time: 22 us; the launch traced here: 21.8 us
  Pallas kernels  19.9 us (90%)
  local copies, waits for them, and re-layouts  1.88 us (9%)
    pallas_call x1, Pallas kernels, shards(): pl.pallas_call(functools.partial(kernel, sizes), out_shape=jax.ShapeDtype...  19.9 us
    unnamed x1, local copies, waits for them, and re-layouts  1.88 us

profile of v1, /device:TPU:17, one launch (start us, length us, event | category | flops | bytes accessed | tf_op | source)
XLA Modules:
  0.0 21.8 jit_solution(15135274843301211757)
XLA Ops:
  0.0 19.9 %shard_map.145 = bf16[2,64,2048]{2,1,0:T(8,128)(2,1)} custom-call(bf16[2,64,2048]{2,1,0:T(8,128)(2,1)} %x_hbm.1, f32[1,2048]{1,0:T(1,128)} %bitcast.18, bf16[2048,512]{1,0:T(8,128)(2,1)} %inw_hbm.1, bf16[2048,512]{1,0:T(8,128)(2,1)} %gw_hbm.1, f32[32,64]{1,0:T(8,128)} %rr_hbm.1, f32[32,64]{1,0:T(8,128)} %ri_hbm.1, f32[1,32]{1,0:T(1,128)} %bitcast.21, ...), custom_call_target="tpu_custom_call" | custom-call | tf_op jit(solution)/shard_map/pallas_call | solution.py:366
  19.9 1.9 %copy.17 = bf16[2,64,2048]{2,1,0:T(8,128)(2,1)} copy(bf16[2,64,2048]{2,1,0:T(8,128)(2,1)} %shard_map.145) | data formatting | bytes 1048576

commit v2 on v1

--- a/solution.py
+++ b/solution.py
@@ -49,7 +49,7 @@
     ng, rr, ri, ls, bre, bim, cre, cim, skip, dec, cg,
     xf, w_in, w_g, w_o, nrm, u_ref, gate_ref, rel_ref,
     bd_re, bd_im, cd_re, cd_im, ti_re, ti_im, to_re, to_im,
-    p_re, p_im, xc_re, xc_im, tot, tot_all, st, st_all, act, act_in,
+    p_re, p_im, xc_re, xc_im, tot, tot_all, st, st_all, act, act_in, chunk_decay, across_re, across_im, acc,
     load_sem, small_sem, tp_send, tp_recv, tot_send, tot_recv, st_send, st_recv,
 ):
     n, tp, S, Q, D, G, N, C, tile_g, out_cols = sizes
@@ -106,22 +106,23 @@
             total = at_end if total is None else total + at_end
             rows = (c * S + s) * Q
             rel_ref[rows:rows + Q, :] = dot(cum - at_mid, to_chan, HIGHEST)
-        totals.append(total)
         tot[s:s + 1, :] = total
 
-    pl.semaphore_wait(barrier, n)
-
-    load_x.wait()
-    load_o.wait()
+    to_mode = (iota((tile_g, mw), 1) // N == iota((tile_g, mw), 0)).astype(F32)
+    logs = jnp.concatenate(mids + lasts, axis=0)
+
+    def widen(rows, q):
+        return jnp.exp(dot(rows[:, q * tile_g:(q + 1) * tile_g], to_mode, HIGHEST))
+
+    for q in range(tiles):
+        chunk_decay[q] = widen(logs, q)
+
     send_x = pltpu.make_async_remote_copy(
         xf.at[me], xf.at[me], tp_send.at[0], tp_recv.at[0], device_id={"tp": peer}, device_id_type=MESH
     )
     send_o = pltpu.make_async_remote_copy(
         w_o.at[me], w_o.at[me], tp_send.at[1], tp_recv.at[1], device_id={"tp": peer}, device_id_type=MESH
     )
-    send_x.start()
-    send_o.start()
-
     def tot_copy(target):
         return pltpu.make_async_remote_copy(
             tot, tot_all.at[sp_me], tot_send.at[target], tot_recv.at[sp_me],
@@ -140,8 +141,6 @@
             return carry
 
         lax.fori_loop(0, n - 1 - sp_me, body, 0)
-
-    to_later(lambda target: tot_copy(target).start())
 
     for copy in small[1:]:
         copy.wait()
@@ -164,8 +163,6 @@
     coef_re = (top_re * rate_re + top_im * rate_im) * inverse
     coef_im = (top_im * rate_re - top_re * rate_im) * inverse
     spread = (iota((N, mw), 1) % N == iota((N, mw), 0)).astype(F32)
-    to_mode = (iota((tile_g, mw), 1) // N == iota((tile_g, mw), 0)).astype(F32)
-
     def rows_of(item, q):
         wide = dot(item[q * tile_g:(q + 1) * tile_g, :], spread, HIGHEST)
         return jnp.sum(wide * to_mode, axis=0, keepdims=True)
@@ -189,6 +186,11 @@
             block = cmul(block, a8)
 
     for q in range(tiles):
+        if q == tiles // 2:
+            pl.semaphore_wait(barrier, n)
+            load_x.wait()
+            send_x.start()
+            to_later(lambda target: tot_copy(target).start())
         a = (rows_of(grown * cosa, q), rows_of(grown * sina, q))
         inv = (rows_of(shrunk * cosa, q), rows_of(-shrunk * sina, q))
         coef = (rows_of(coef_re, q), rows_of(coef_im, q))
@@ -218,6 +220,8 @@
         rows = pl.ds(pl.multiple_of(first, SQ), SQ)
         u_ref[rows, :] = dot(nrm[rows, :], w_in[...]).astype(BF16)
 
+    load_o.wait()
+    send_o.start()
     load_in.wait()
     project(me)
     send_x.wait_recv()
@@ -237,17 +241,15 @@
         p_re[q] = dot(chunk_tri, z_re.reshape(R, mw).astype(BF16))
         p_im[q] = dot(chunk_tri, z_im.reshape(R, mw).astype(BF16))
 
-    def widen(row, q):
-        return jnp.exp(dot(jnp.broadcast_to(row[:, q * tile_g:(q + 1) * tile_g], (8, tile_g)), to_mode, HIGHEST)[0:1])
-
     enter_f, leave_f = {}, {}
     for q in range(tiles):
         for s in range(S):
             x = None
             for c in range(tp):
                 b = c * S + s
-                e_mid = widen(mids[s * tp + c], q)
-                e_end = widen(lasts[s * tp + c], q)
+                k = s * tp + c
+                e_mid = chunk_decay[q, k:k + 1, :]
+                e_end = chunk_decay[q, S * tp + k:S * tp + k + 1, :]
                 enter_f[q, s, c] = (up_half[q][0] * e_mid, up_half[q][1] * e_mid)
                 leave_f[q, s, c] = (up_end[q][0] * e_end, up_end[q][1] * e_end)
                 last = b * Q + Q - 1
@@ -264,19 +266,27 @@
     load_g.wait()
     gate_ref[...] = dot(nrm[...], w_g[...]).astype(BF16)
 
-    def enter(j, x):
+    def tot_here(j, carry):
         pltpu.make_async_remote_copy(
             tot, tot_all.at[j], tot_send.at[j], tot_recv.at[j], device_id={"tp": peer}, device_id_type=MESH
         ).wait_recv()
+        return carry
+
+    lax.fori_loop(0, sp_me, tot_here, 0)
+    all_logs = tot_all[...].reshape(n * 8, G)
+    for q in range(tiles):
+        decay = widen(all_logs, q)
+        across_re[:, q] = (up_all[q][0] * decay).reshape(n, 8, mw)
+        across_im[:, q] = (up_all[q][1] * decay).reshape(n, 8, mw)
+
+    def enter(j, x):
         pltpu.make_async_remote_copy(
             st, st_all.at[j], st_send.at[j], st_recv.at[j], device_id={"tp": peer}, device_id_type=MESH
         ).wait_recv()
-        logs = tot_all[j]
         new = []
         for q in range(tiles):
-            decay = jnp.exp(dot(logs[:, q * tile_g:(q + 1) * tile_g], to_mode, HIGHEST))[0:S]
             got = st_all[j, q].astype(F32)
-            re, im = cmul((up_all[q][0] * decay, up_all[q][1] * decay), x[q])
+            re, im = cmul((across_re[j, q, 0:S], across_im[j, q, 0:S]), x[q])
             new.append((re + got[0:S], im + got[S:2 * S]))
         return tuple(new)
 
@@ -328,6 +338,9 @@
     own = act[me].astype(F32)
     own_sq = jnp.sum(own * own, axis=-1, keepdims=True)
     own_g = (own * cg[me]).astype(BF16)
+    for k in range(D // out_cols):
+        cols = slice(k * out_cols, (k + 1) * out_cols)
+        acc[:, cols] = dot(own_g, w_o[me, :, cols])
     send_o.wait_recv()
     send_a.wait_recv()
     got = act_in[...].astype(F32)
@@ -336,7 +349,7 @@
     scale = lax.rsqrt((own_sq + got_sq) * (1.0 / (tp * W)) + epsilon)
     for k in range(D // out_cols):
         cols = slice(k * out_cols, (k + 1) * out_cols)
-        y = dot(own_g, w_o[me, :, cols]) + dot(got_g, w_o[peer, :, cols])
+        y = acc[:, cols] + dot(got_g, w_o[peer, :, cols])
         out[:, :, cols] = (y * scale).astype(BF16).reshape(S, Q, out_cols)
 
     send_x.wait_send()
@@ -406,6 +419,10 @@
             pltpu.VMEM((n, tiles, 2 * S, mw), BF16),
             pltpu.VMEM((tp, S * Q, W), BF16),
             pltpu.VMEM((S * Q, W), BF16),
+            pltpu.VMEM((tiles, 2 * S * tp, mw), F32),
+            pltpu.VMEM((n, tiles, 8, mw), F32),
+            pltpu.VMEM((n, tiles, 8, mw), F32),
+            pltpu.VMEM((S * Q, D), F32),
             dma((4,)),
             dma((11,)),
             dma((3,)),

time: 22 us -> 19.6 us (0.89)
  Pallas kernels: 19.9 us -> 17.5 us
    pallas_call x1, Pallas kernels: 19.9 us -> 17.5 us  [shards(): pl.pallas_call(functools.partial(kernel, sizes), out_shape=jax.ShapeDtype...]
where the time goes in v2:
time: 19.6 us; the launch traced here: 19.4 us
  Pallas kernels  17.5 us (89%)
  local copies, waits for them, and re-layouts  1.88 us (10%)
    pallas_call x1, Pallas kernels, shards(): pl.pallas_call(functools.partial(kernel, sizes), out_shape=jax.ShapeDtype...  17.5 us
    unnamed x1, local copies, waits for them, and re-layouts  1.88 us

profile of v2, /device:TPU:17, one launch (start us, length us, event | category | flops | bytes accessed | tf_op | source)
XLA Modules:
  0.0 19.4 jit_solution(12621580955715535603)
XLA Ops:
  0.0 17.5 %shard_map.145 = bf16[2,64,2048]{2,1,0:T(8,128)(2,1)} custom-call(bf16[2,64,2048]{2,1,0:T(8,128)(2,1)} %x_hbm.1, f32[1,2048]{1,0:T(1,128)} %bitcast.18, bf16[2048,512]{1,0:T(8,128)(2,1)} %inw_hbm.1, bf16[2048,512]{1,0:T(8,128)(2,1)} %gw_hbm.1, f32[32,64]{1,0:T(8,128)} %rr_hbm.1, f32[32,64]{1,0:T(8,128)} %ri_hbm.1, f32[1,32]{1,0:T(1,128)} %bitcast.21, ...), custom_call_target="tpu_custom_call" | custom-call | tf_op jit(solution)/shard_map/pallas_call | solution.py:379
  17.5 1.9 %copy.17 = bf16[2,64,2048]{2,1,0:T(8,128)(2,1)} copy(bf16[2,64,2048]{2,1,0:T(8,128)(2,1)} %shard_map.145) | data formatting | bytes 1048576
